TPU v7x, 512 devices: a whole 4x8x8 slice. The times are simulated.
512 devices in a mesh: ep: 32 (over z, x), tp: 16 (over y, core).
Axes of the slice: x: 4, y: 8, z: 8, core: 2. Of those that a mesh axis runs over, the one named last changes fastest.
Arguments:
- mixer_query: bfloat16 [8192, 2048], P('ep', 'tp'), may hold values from -6 to 6
- mixer_forget: bfloat16 [8192, 2048], P('ep', 'tp'), may hold values from -5.5 to 5.5
- mixer_value: bfloat16 [8192, 2048], P('ep', 'tp'), may hold values from -6 to 6
- mixer_gate: bfloat16 [8192, 2048], P('ep', 'tp'), may hold values from -6 to 6
- forget_floor: float32 [2048], P('tp'), may hold values from 0.88 to 1
- head_gain: float32 [128], replicated, may hold values from 0.1 to 1.9
- mixer_proj: bfloat16 [2048, 2048], P(None, 'tp'), may hold values from -0.125 to 0.125
- expert_tokens: bfloat16 [4096, 2048], P('ep'), may hold values from -6 to 6
- expert_gain: float32 [2048], replicated, may hold values from 0.1 to 1.9
- routes: int32 [4096, 2], P('ep'), may hold values from 0 to 31, as said below
- group_logits: float32 [4096, 4], P('ep'), may hold values from -6 to 6
- choice_logits: float32 [4096, 2], P('ep'), may hold values from -6 to 6
- w_gate: bfloat16 [32, 2048, 2048], P('ep', None, 'tp'), may hold values from -0.125 to 0.125
- w_up: bfloat16 [32, 2048, 2048], P('ep', None, 'tp'), may hold values from -0.125 to 0.125
- w_down: bfloat16 [32, 2048, 2048], P('ep', None, 'tp'), may hold values from -0.125 to 0.125
Outputs:
- mixer_out: bfloat16 [8192, 2048], P('ep', 'tp')
- expert_out: bfloat16 [4096, 2048], P('ep', 'tp')
Inputs may be any that keep to these rules, and one draw needn't show every extreme that they name: `routes`: in each aligned block of 128 rows (the rows of one index of ep) no expert is named by more than 16 rows, and some expert reaches that bound in every block; the 2 experts of a row differ and lie in the same group.
All inputs are finite; a program needn't handle non-finite values.
Results may differ from a plain program's by a relative error of at most 0.01.
Values may be sent and summed in bfloat16 or wider, within the bound.
A program may use at most 64 MiB of HBM per device.

v0:
```python
import jax
import jax.numpy as jnp
from jax import lax
from jax.sharding import Mesh
from jax.sharding import PartitionSpec as P

KEYDIM = 128
VDIM = 128
GROUPS = 4
TOPK = 2
BLOCK = 64
EP = ("ep_0", "ep_1")


norm_eps = 1e-06
highest_precision = lax.Precision.HIGHEST


def filled_with(shard, identity):
    return jax.tree.map(
        lambda part, zero: jnp.zeros_like(part) + jnp.asarray(zero, part.dtype), shard, identity
    )


def collected_together(shard, axis):
    leaves = jax.tree.leaves(shard)
    sequence = sorted(range(len(leaves)), key=lambda k: -leaves[k].size)
    width = (1, *leaves[sequence[0]].shape)[-1]
    lines = [
        jnp.pad(leaves[k].reshape(-1), (0, -leaves[k].size % width)).reshape(-1, width)
        for k in sequence
    ]
    both, at, found = (lax.all_gather(jnp.concatenate(lines), axis), 0, {})
    for k, line in zip(sequence, lines):
        section = both[:, at : at + len(line)].reshape(len(both), -1)
        found[k] = section[:, : leaves[k].size].reshape(-1, *leaves[k].shape)
        at += len(line)
    numbers = iter(range(len(leaves)))
    return jax.tree.map(lambda _: found[next(numbers)], shard)


def carried_in(shard, axes, combine, identity):
    before = start = filled_with(shard, identity)
    so_far = shard
    for axis in reversed(axes):
        devices, index = (lax.axis_size(axis), lax.axis_index(axis))
        pieces = collected_together(
            jax.tree.map(
                lambda part, kind: part.astype(kind), so_far, (jnp.bfloat16, jnp.bfloat16)
            ),
            axis,
        )
        inside, so_far = (start, start)
        for k in range(devices):
            passed = k < index
            so_far = combine(
                so_far, jax.tree.map(lambda part, own: part[k].astype(own.dtype), pieces, shard)
            )
            inside = jax.tree.map(lambda new, old: jnp.where(passed, new, old), so_far, inside)
        before = combine(inside, before)
    return before


def laid_out(pieces, dim):
    dims = list(pieces.shape[1:])
    dims[dim] *= pieces.shape[0]
    return jnp.moveaxis(pieces, 0, dim).reshape(dims)


def from_everyone(shard, axis):
    copies = jnp.broadcast_to(shard, (lax.axis_size(axis), *shard.shape))
    return lax.all_to_all(copies, axis, split_axis=0, concat_axis=0, tiled=True)


def gather_directly(shard, axis, dim):
    return laid_out(from_everyone(shard, axis), dim)


def rms_scale(features, gain_vec):
    return (
        features
        * lax.rsqrt(jnp.mean(features * features, axis=-1, keepdims=True) + norm_eps)
        * gain_vec
    )


def block_terms(query_block, input_block, log_blk, value_block, carried_state):
    cumulative_log = jnp.cumsum(log_blk, axis=0)
    between_block_term = jnp.einsum(
        "zug,ugr->zur",
        query_block * jnp.exp(cumulative_log),
        carried_state,
        precision=highest_precision,
    )
    causal = jnp.tril(jnp.ones((query_block.shape[0], query_block.shape[0]), dtype=bool))[
        :, :, None, None
    ]
    differ = cumulative_log[:, None] - cumulative_log[None, :]
    decays = jnp.exp(jnp.where(causal, differ, -jnp.inf))
    scores = jnp.sum(query_block[:, None] * input_block[None, :] * decays, axis=-1)
    result = between_block_term + jnp.einsum(
        "tsh,shv->thv", scores, value_block, precision=highest_precision
    )
    ending_log_decay = cumulative_log[-1]
    updated_state = jnp.exp(ending_log_decay)[..., None] * carried_state + jnp.einsum(
        "twa,twr->war",
        input_block * jnp.exp(ending_log_decay[None] - cumulative_log),
        value_block,
        precision=highest_precision,
    )
    return (updated_state, result, cumulative_log)


def mixer_local(
    mixer_query, mixer_forget, mixer_value, mixer_gate, forget_floor, head_gain, mixer_proj
):
    length = mixer_query.shape[0]
    heads_local = mixer_query.shape[1] // KEYDIM
    blocks = length // BLOCK

    def split_blocks(source_array, last_width):
        return source_array.reshape(blocks, BLOCK, heads_local, last_width)

    queries = jax.nn.silu(mixer_query.astype(jnp.float32))
    input_rates = (1.0 - forget_floor) * jax.nn.sigmoid(-mixer_forget.astype(jnp.float32))
    log_forget = jnp.log1p(-input_rates)
    value_rows = mixer_value.astype(jnp.float32)

    def advance(carry_pair, block_inputs):
        carried_state, offset_log = carry_pair
        query_block, input_block, value_block, log_blk = block_inputs
        updated_state, result, cumulative_log = block_terms(
            query_block, input_block, log_blk, value_block, carried_state
        )
        scaled_values = query_block * jnp.exp(cumulative_log + offset_log[None])
        return ((updated_state, offset_log + cumulative_log[-1]), (result, scaled_values))

    initial = (
        jnp.zeros((heads_local, KEYDIM, VDIM), jnp.float32),
        jnp.zeros((heads_local, KEYDIM), jnp.float32),
    )
    (local_state, total_log), (output_rows, scaled_values) = lax.scan(
        advance,
        initial,
        (
            split_blocks(queries, KEYDIM),
            split_blocks(input_rates, KEYDIM),
            split_blocks(value_rows, VDIM),
            split_blocks(log_forget, KEYDIM),
        ),
    )

    def combine(earlier, later):
        return (earlier[0] * later[0], later[0][..., None] * earlier[1] + later[1])

    identity = (jnp.ones_like(total_log), jnp.zeros_like(local_state))
    incoming_state = carried_in((jnp.exp(total_log), local_state), EP, combine, identity)
    output_rows = output_rows + jnp.einsum(
        "qsfa,fap->qsfp", scaled_values, incoming_state[1], precision=highest_precision
    )
    output_rows = output_rows.reshape(length, heads_local, VDIM)
    gate_act = jax.nn.silu(mixer_gate.astype(jnp.float32)).reshape(length, heads_local, VDIM)
    gated_out = rms_scale(output_rows, head_gain) * gate_act
    mixed_heads = gated_out.reshape(length, heads_local * VDIM).astype(jnp.bfloat16)
    summed = jnp.dot(
        lax.all_gather(mixed_heads, "tp", axis=1, tiled=True),
        mixer_proj,
        preferred_element_type=jnp.float32,
    )
    return summed.astype(jnp.bfloat16)


def gate_weights(routes, group_logits, choice_logits, group_size):
    group_exp = jnp.exp(group_logits)
    group_prob = group_exp / jnp.sum(group_exp, axis=-1, keepdims=True)
    groups_of = routes // group_size
    member = (groups_of[..., None] == jnp.arange(GROUPS, dtype=jnp.int32)).astype(jnp.float32)
    picked_prob = jnp.sum(member * group_prob[:, None, :], axis=-1)
    choice_exp = jnp.exp(choice_logits)
    together = (groups_of[:, :, None] == groups_of[:, None, :]).astype(jnp.float32)
    within = jnp.sum(together * choice_exp[:, None, :], axis=-1)
    return picked_prob * choice_exp / within


def finish(gate_pre, up_pre, down_local, sources, slot_count):
    hidden = (jax.nn.silu(gate_pre) * up_pre).astype(jnp.bfloat16)
    summed = jnp.dot(
        gather_directly(hidden, "tp", 1), down_local, preferred_element_type=jnp.float32
    )
    shaped = summed.astype(jnp.bfloat16).reshape(sources, slot_count, down_local.shape[1])
    return lax.all_to_all(shaped, EP, split_axis=0, concat_axis=0, tiled=True)


def expert_local(
    expert_tokens, expert_gain, routes, group_logits, choice_logits, w_gate, w_up, w_down
):
    count_rows, model_width = expert_tokens.shape
    experts_all = lax.axis_size(EP)
    capacity = 2 * TOPK * count_rows // experts_all
    normed = rms_scale(expert_tokens.astype(jnp.float32), expert_gain).astype(jnp.bfloat16)
    weights = gate_weights(routes, group_logits, choice_logits, experts_all // GROUPS)
    flat_routes = routes.reshape(-1)
    onehot = (flat_routes[:, None] == jnp.arange(experts_all, dtype=jnp.int32)).astype(jnp.int32)
    earlier = jnp.cumsum(onehot, axis=0) - onehot
    ranks = jnp.sum(earlier * onehot, axis=-1)
    slot_of = flat_routes * capacity + ranks
    token_ids = jnp.arange(flat_routes.shape[0], dtype=jnp.int32) // TOPK
    token_of = jnp.full((experts_all * capacity,), count_rows, jnp.int32).at[slot_of].set(token_ids)
    padded = jnp.concatenate([normed, jnp.zeros((1, model_width), jnp.bfloat16)], axis=0)
    outgoing = padded[token_of].reshape(experts_all, capacity, model_width)
    gate_local = w_gate[0]
    up_local = w_up[0]
    down_local = w_down[0]
    arrived = lax.all_to_all(outgoing, EP, split_axis=0, concat_axis=0, tiled=True)
    sources, slot_count, _ = arrived.shape
    flat_in = arrived.reshape(sources * slot_count, model_width)
    gate_pre = jnp.dot(flat_in, gate_local, preferred_element_type=jnp.float32)
    up_pre = jnp.dot(flat_in, up_local, preferred_element_type=jnp.float32)
    came_back = finish(gate_pre, up_pre, down_local, sources, slot_count)
    picked = (
        came_back.reshape(-1, came_back.shape[-1])[slot_of].astype(jnp.float32)
        * weights.reshape(-1)[:, None]
    )
    return jnp.sum(picked.reshape(count_rows, TOPK, -1), axis=1).astype(jnp.bfloat16)


def per_device(
    mixer_query,
    mixer_forget,
    mixer_value,
    mixer_gate,
    forget_floor,
    head_gain,
    mixer_proj,
    expert_tokens,
    expert_gain,
    routes,
    group_logits,
    choice_logits,
    w_gate,
    w_up,
    w_down,
):
    mixer_out = mixer_local(
        mixer_query, mixer_forget, mixer_value, mixer_gate, forget_floor, head_gain, mixer_proj
    )
    expert_out = expert_local(
        expert_tokens, expert_gain, routes, group_logits, choice_logits, w_gate, w_up, w_down
    )
    return (mixer_out, expert_out)


def solution(mesh):
    finer = Mesh(mesh.devices.reshape(8, 4, mesh.shape["tp"]), ("ep_0", "ep_1", "tp"))
    placed = (
        P(EP, "tp"),
        P(EP, "tp"),
        P(EP, "tp"),
        P(EP, "tp"),
        P("tp"),
        P(),
        P(None, "tp"),
        P(EP, None),
        P(),
        P(EP, None),
        P(EP, None),
        P(EP, None),
        P(EP, None, "tp"),
        P(EP, None, "tp"),
        P(EP, None, "tp"),
    )
    return jax.shard_map(
        per_device,
        mesh=finer,
        in_specs=placed,
        out_specs=(P(EP, "tp"), P(EP, "tp")),
        check_vma=False,
    )
```

profile of v0, /device:TPU:1, one launch (start us, length us, event | category | flops | bytes accessed | tf_op | source)
XLA Modules:
  0.0 173.8 jit_solution(17011988294751444505)
XLA Ops:
  7.2 0.0 copy-start
  7.2 0.8 copy.50
  8.0 0.1 eq.55
  8.2 0.1 eq.51
  8.3 0.7 and_select_fusion
  9.0 0.6 reduce-window.6
  9.6 0.2 slice_reduce_fusion
  9.8 0.1 copy.49
  10.0 0.1 mul.434
  10.1 0.1 fusion.84
  10.2 1.4 scatter_custom_fusion
  11.6 1.2 fusion.24
  12.9 1.2 fusion.26
  14.2 3.3 %gather_fusion = bf16[512,2048]{1,0:T(8,128)(2,1)} fusion(bf16[129,2048]{1,0:T(8,128)(2,1)S(1)} %concatenate.11, s32[1024]{0:T(1024)S(1)} %pad_clamp_fusion.1), kind=kCustom, calls=%fused_computation | custom fusion | bytes 4196352 | tf_op jit(solution)/shard_map/gather | solution.py:210
  17.5 13.8 %all-to-all-start = ((bf16[32,16,2048]{2,1,0:T(8,128)(2,1)}), bf16[32,16,2048]{2,1,0:T(8,128)(2,1)S(1)}, u32[]{:S(2)}, u32[]{:S(2)}) async-start(bf16[32,16,2048]{2,1,0:T(8,128)(2,1)} %bitcast.31), calls=%async_computation | async-start | bytes 4194304 | tf_op jit(solution)/shard_map/all_to_all | solution.py:214
  31.5 0.1 divide_multiply_fusion
  31.6 13.7 %while.17 = (s32[]{:T(128)}, f32[1,128,128]{2,1,0:T(8,128)S(1)}, f32[1,128]{1,0:T(1,128)S(1)}, f32[4,64,1,128]{3,1,2,0:T(8,128)}, f32[4,64,1,128]{3,1,2,0:T(8,12...) while((s32[]{:T(128)}, f32[1,128,128]{2,1,0:T(8,128)S(1)}, ...), condition=%wide.region_3.4_spmd.clone, body=%wide.region_0.3_spmd.clone.sunk | while | flops 34709760 | bytes 1030797 | solution.py:142
  31.7 0.1 fusion.169
  31.8 0.6 multiply_dynamic-update-slice_fusion.2
  32.4 1.4 multiply_reduce_fusion.3
  33.7 0.2 convolution_bitcast_fusion.4
  34.0 0.8 fusion.173
  34.7 0.3 fusion.171
  35.1 0.1 fusion.169
  35.2 0.6 multiply_dynamic-update-slice_fusion.2
  35.8 1.4 multiply_reduce_fusion.3
  37.2 0.2 convolution_bitcast_fusion.4
  37.4 0.8 fusion.173
  38.2 0.3 fusion.171
  38.5 0.1 fusion.169
  38.6 0.6 multiply_dynamic-update-slice_fusion.2
  39.2 1.4 multiply_reduce_fusion.3
  40.6 0.2 convolution_bitcast_fusion.4
  40.8 0.8 fusion.173
  41.6 0.3 fusion.171
  41.9 0.1 fusion.169
  42.0 0.6 multiply_dynamic-update-slice_fusion.2
  42.7 1.4 multiply_reduce_fusion.3
  44.0 0.2 convolution_bitcast_fusion.4
  44.2 0.8 fusion.173
  45.0 0.3 fusion.171
  45.4 0.0 copy-start.9
  45.4 10.6 %all-gather.2 = bf16[4,129,128]{2,1,0:T(8,128)(2,1)S(1)} all-gather(bf16[1,129,128]{2,1,0:T(8,128)(2,1)S(1)} %maximum_bitcast_fusion), channel_id=2, replica_groups=mesh['ep_0'=8,'ep_1'=4,'tp'=16] {'ep_1'}, dimensions={0}, use_global_device_ids=true | all-gather | bytes 165120 | tf_op jit(solution)/shard_map/all_gather | solution.py:33
  56.0 23.8 %all-to-all-done = bf16[32,16,2048]{2,1,0:T(8,128)(2,1)S(1)} async-done(((bf16[32,16,2048]{2,1,0:T(8,128)(2,1)}), bf16[32,16,2048]{2,1,0:T(8,128)(2,1)S(1)}, u32[]{:S(2)}, u32[]{:S(2)}) %all-to-all-start) | async-done | bytes 2097184 | tf_op jit(solution)/shard_map/all_to_all | solution.py:214
  79.9 0.7 fusion.29
  80.6 0.7 fusion.22
  81.3 0.1 copy.53
  81.4 1.6 broadcast_in_dim.37
  83.0 9.9 %all-to-all-start.1 = ((bf16[16,512,128]{1,2,0:T(8,128)(2,1)}), bf16[16,512,128]{1,2,0:T(8,128)(2,1)S(1)}, u32[]{:S(2)}, u32[]{:S(2)}) async-start(bf16[16,512,128]{1,2,0:T(8,128)(2,1)} %broadcast_in_dim.37), calls=%async_computation.1 | async-start | bytes 4194304 | tf_op jit(solution)/shard_map/all_to_all | solution.py:72
  92.9 0.0 all-gather.6.cloned.1.call-start
  93.0 0.1 fusion.81
  93.1 20.6 %all-gather.3 = bf16[8,129,128]{2,1,0:T(8,128)(2,1)S(1)} all-gather(bf16[1,129,128]{2,1,0:T(8,128)(2,1)S(1)} %maximum_bitcast_fusion.1), channel_id=3, replica_groups=mesh['ep_0'=8,'ep_1'=4,'tp'=16] {'ep_0'}, dimensions={0}, use_global_device_ids=true | all-gather | bytes 297216 | tf_op jit(solution)/shard_map/all_gather | solution.py:33
  113.8 1.7 multiply_reduce_fusion.1
  115.5 0.1 rsqrt.20
  115.6 0.7 fusion.41
  116.3 0.0 all-gather.6.cloned.1.call-update
  116.4 0.1 copy.54
  116.6 26.2 %all-to-all-done.1 = bf16[16,512,128]{1,2,0:T(8,128)(2,1)S(1)} async-done(((bf16[16,512,128]{1,2,0:T(8,128)(2,1)}), bf16[16,512,128]{1,2,0:T(8,128)(2,1)S(1)}, u32[]{:S(2)}, u32[]{:S(2)}) %all-to-all-start.1) | async-done | bytes 2097184 | tf_op jit(solution)/shard_map/all_to_all | solution.py:72
  142.8 2.4 %convolution_convert_fusion = bf16[512,128]{1,0:T(8,128)(2,1)} fusion(bf16[512,2048]{0,1:T(8,128)(2,1)S(1)} %bitcast.225, bf16[1,2048,128]{2,1,0:T(8,128)(2,1)} %param.31), kind=kOutput, calls=%fused_computation.42 | convolution fusion | flops 268500992 | bytes 2752512 | tf_op jit(solution)/shard_map/dot_general | solution.py:187
  145.2 5.1 %all-to-all-start.2 = ((bf16[32,16,128]{2,1,0:T(8,128)(2,1)}), bf16[32,16,128]{2,1,0:T(8,128)(2,1)S(1)}, u32[]{:S(2)}, u32[]{:S(2)}) async-start(bf16[32,16,128]{2,1,0:T(8,128)(2,1)} %bitcast.38), calls=%async_computation.2 | async-start | bytes 262144 | tf_op jit(solution)/shard_map/all_to_all | solution.py:191
  150.3 12.6 %all-gather.6.cloned.1.call-done = bf16[256,2048]{1,0:T(8,128)(2,1)} async-done(((bf16[256,128]{1,0:T(8,128)(2,1)}), bf16[256,2048]{1,0:T(8,128)(2,1)}) %all-gather.6.cloned.1.call-update) | async-done | bytes 1048592 | tf_op jit(solution)/shard_map/all_gather | solution.py:166
  162.9 2.3 %convolution_convert_fusion.1 = bf16[256,128]{1,0:T(8,128)(2,1)} fusion(bf16[256,2048]{1,0:T(8,128)(2,1)} %all-gather.6.cloned.1.call-done, bf16[2048,128]{1,0:T(8,128)(2,1)S(1)} %copy-done.1), kind=kOutput, calls=%fused_computation.45 | convolution fusion | flops 134250496 | bytes 1638400 | tf_op jit(solution)/shard_map/dot_general | solution.py:165
  165.2 0.9 gather_fusion.1
  166.1 0.9 fusion.38
  (82 shorter events, 0.6 us)
Async XLA Ops:
  7.2 72.7 %copy-start = (bf16[1,2048,128]{2,1,0:T(8,128)(2,1)S(1)}, bf16[1,2048,128]{2,1,0:T(8,128)(2,1)}, u32[]{:S(2)}) copy-start(bf16[1,2048,128]{2,1,0:T(8,128)(2,1)} %param.29) | copy-start | bytes 1572868
  17.5 13.9 %copy-start.10 = (f32[128]{0:T(128)S(1)}, f32[128]{0:T(128)}, u32[]{:S(2)}) copy-start(f32[128]{0:T(128)} %param.21) | copy-start | bytes 1540
  17.5 13.9 %copy-start.2 = (bf16[256,128]{1,0:T(8,128)(2,1)S(1)}, bf16[256,128]{1,0:T(8,128)(2,1)}, u32[]{:S(2)}) copy-start(bf16[256,128]{1,0:T(8,128)(2,1)} %param.19) | copy-start | bytes 196612
  17.5 14.0 %copy-start.3 = (bf16[256,128]{1,0:T(8,128)(2,1)S(1)}, bf16[256,128]{1,0:T(8,128)(2,1)}, u32[]{:S(2)}) copy-start(bf16[256,128]{1,0:T(8,128)(2,1)} %param.17) | copy-start | bytes 196612
  17.5 14.0 %copy-start.4 = (bf16[256,128]{1,0:T(8,128)(2,1)S(1)}, bf16[256,128]{1,0:T(8,128)(2,1)}, u32[]{:S(2)}) copy-start(bf16[256,128]{1,0:T(8,128)(2,1)} %param.18) | copy-start | bytes 196612
  17.5 62.3 %all-to-all-start = ((bf16[32,16,2048]{2,1,0:T(8,128)(2,1)}), bf16[32,16,2048]{2,1,0:T(8,128)(2,1)S(1)}, u32[]{:S(2)}, u32[]{:S(2)}) async-start(bf16[32,16,2048]{2,1,0:T(8,128)(2,1)} %bitcast.31), calls=%async_computation | async-start | bytes 4194304 | tf_op jit(solution)/shard_map/all_to_all | solution.py:214
  45.4 35.2 %copy-start.9 = (bf16[1,2048,128]{2,1,0:T(8,128)(2,1)S(1)}, bf16[1,2048,128]{2,1,0:T(8,128)(2,1)}, u32[]{:S(2)}) copy-start(bf16[1,2048,128]{2,1,0:T(8,128)(2,1)} %param.30) | copy-start | bytes 1572868
  83.0 32.6 %copy-start.5 = (bf16[256,128]{1,0:T(8,128)(2,1)S(1)}, bf16[256,128]{1,0:T(8,128)(2,1)}, u32[]{:S(2)}) copy-start(bf16[256,128]{1,0:T(8,128)(2,1)} %param.20) | copy-start | bytes 196612
  83.0 32.6 %copy-start.8 = (f32[128]{0:T(128)S(1)}, f32[128]{0:T(128)}, u32[]{:S(2)}) copy-start(f32[128]{0:T(128)} %param.22) | copy-start | bytes 1540
  83.0 59.8 %all-to-all-start.1 = ((bf16[16,512,128]{1,2,0:T(8,128)(2,1)}), bf16[16,512,128]{1,2,0:T(8,128)(2,1)S(1)}, u32[]{:S(2)}, u32[]{:S(2)}) async-start(bf16[16,512,128]{1,2,0:T(8,128)(2,1)} %broadcast_in_dim.37), calls=%async_computation.1 | async-start | bytes 4194304 | tf_op jit(solution)/shard_map/all_to_all | solution.py:72
  92.9 23.5 %copy-start.7 = (f32[128,2]{0,1:T(2,128)S(1)}, f32[128,2]{0,1:T(2,128)}, u32[]{:S(2)}) copy-start(f32[128,2]{0,1:T(2,128)} %param.28) | copy-start | bytes 3076
  92.9 23.5 %copy-start.6 = (f32[128,4]{0,1:T(4,128)S(1)}, f32[128,4]{0,1:T(4,128)}, u32[]{:S(2)}) copy-start(f32[128,4]{0,1:T(4,128)} %param.27) | copy-start | bytes 6148
  92.9 70.0 %all-gather.6.cloned.1.call-start = ((), (), s32[]{:S(2)}) async-start(), calls=%async_computation.3 | async-start | bytes 1114112 | tf_op jit(solution)/shard_map/all_gather | solution.py:166
  113.8 49.2 %copy-start.1 = (bf16[2048,128]{1,0:T(8,128)(2,1)S(1)}, bf16[2048,128]{1,0:T(8,128)(2,1)}, u32[]{:S(2)}) copy-start(bf16[2048,128]{1,0:T(8,128)(2,1)} %param.23) | copy-start | bytes 1572868
  145.2 20.0 %all-to-all-start.2 = ((bf16[32,16,128]{2,1,0:T(8,128)(2,1)}), bf16[32,16,128]{2,1,0:T(8,128)(2,1)S(1)}, u32[]{:S(2)}, u32[]{:S(2)}) async-start(bf16[32,16,128]{2,1,0:T(8,128)(2,1)} %bitcast.38), calls=%async_computation.2 | async-start | bytes 262144 | tf_op jit(solution)/shard_map/all_to_all | solution.py:191
Sparse Core Ops, SparseCore 0:
  116.4 46.4 all-gather.5
where the time goes:
time: 174 us
  waiting for transfers between devices  62.6 us (36%)
  blocking collectives  31.2 us (18%)
  starting transfers between devices  28.9 us (17%)
  between operations  14.4 us (8%)
  other arithmetic  14.2 us (8%)
  matrix products  12.9 us (7%)
  local copies, waits for them, and re-layouts  9.24 us (5%)
    all_gather x2, blocking collectives, collected_together(): both, at, found = (lax.all_gather(jnp.concatenate(lines), axis), 0, {})  31.2 us
    all_to_all x1, waiting for transfers between devices, from_everyone(): return lax.all_to_all(copies, axis, split_axis=0, concat_axis=0, tiled=True)  26.2 us
    all_to_all x1, waiting for transfers between devices, expert_local(): lax.all_to_all(outgoing, EP, split_axis=0, concat_axis=0, tiled=True)  23.8 us
    all_to_all x1, starting transfers between devices, expert_local(): lax.all_to_all(outgoing, EP, split_axis=0, concat_axis=0, tiled=True)  13.8 us
    all_gather x1, waiting for transfers between devices, mixer_local(): lax.all_gather(mixed_heads, 'tp', axis=1, tiled=True)  12.6 us
    all_to_all x1, starting transfers between devices, from_everyone(): return lax.all_to_all(copies, axis, split_axis=0, concat_axis=0, tiled=True)  9.89 us
    reduce_sum x4, other arithmetic, block_terms(): jnp.sum(query_block[:, None] * input_block[None, :] * decays, axis=-1)  5.4 us
    all_to_all x1, starting transfers between devices, finish(): return lax.all_to_all(shaped, EP, split_axis=0, concat_axis=0, tiled=True)  5.08 us
  transfers between devices with their start and end apart: 4, of which 3 were waited for; matrix products, arithmetic and copies ran while one was open for 12% of the time, Pallas kernels for 0%

commit v1 on v0

v1 whole, which is shorter than its diff:
```python
import jax
import jax.numpy as jnp
from jax import lax
from jax.experimental import pallas as pl
from jax.experimental.pallas import tpu as pltpu
from jax.sharding import Mesh
from jax.sharding import PartitionSpec as P

NZ, NX, NY, NC = 8, 4, 8, 2
EXPERTS = NZ * NX
TP = NY * NC
GROUPS = 4
EXP_GROUP = EXPERTS // GROUPS
CAP = 16
SLOTS = EXPERTS * CAP
LANES = 128
TOKENS_A = 256
TOKENS_B = 128
WIDTH = 2048
CHUNK = 128
MSG = 48
SLICE = LANES // NX
MESH = pl.DeviceIdType.MESH
norm_eps = 1e-06

f32, bf16, i32 = jnp.float32, jnp.bfloat16, jnp.int32


def remote(src, dst, send_sem, recv_sem, **where):
    return pltpu.make_async_remote_copy(
        src_ref=src,
        dst_ref=dst,
        send_sem=send_sem,
        recv_sem=recv_sem,
        device_id=where,
        device_id_type=MESH,
    )


def drain(view, sem):
    pltpu.make_async_copy(view, view, sem).wait()


def sigmoid(v):
    return jax.nn.sigmoid(v)


def halves(v):
    high = v.astype(bf16)
    return high, (v - high.astype(f32)).astype(bf16)


def nn(a, b):
    return lax.dot_general(a, b, (((1,), (0,)), ((), ())), preferred_element_type=f32)


def nt(a, b):
    return lax.dot_general(a, b, (((1,), (1,)), ((), ())), preferred_element_type=f32)


class Ring:
    def __init__(self, buf, sems, y, c):
        self.buf, self.y, self.c = buf, y, c
        self.send, self.from_left, self.from_right, self.pair_send, self.pair_recv = sems
        self.chunks = buf.shape[1] // CHUNK
        self.right, self.left = lax.rem(y + 1, NY), lax.rem(y + NY - 1, NY)

    def at(self, chip, q):
        return self.buf.at[chip * NC + self.c, pl.ds(q * CHUNK, CHUNK)]

    def reach(self, q):
        return (4, 3) if q % 2 == 0 else (3, 4)

    def go_right(self, chip, hop, q):
        v = self.at(chip, q)
        return remote(v, v, self.send.at[0], self.from_left.at[hop, q], y=self.right)

    def go_left(self, chip, hop, q):
        v = self.at(chip, q)
        return remote(v, v, self.send.at[0], self.from_right.at[hop, q], y=self.left)

    def pair(self, chip, q):
        v = self.at(chip, q)
        return remote(v, v, self.pair_send.at[0], self.pair_recv.at[q], c=1 - self.c)

    def start(self, q):
        self.go_right(self.y, 0, q).start()
        self.go_left(self.y, 0, q).start()
        self.pair(self.y, q).start()

    def step(self, hop, q):
        to_right, to_left = self.reach(q)
        if hop <= to_right:
            chip = lax.rem(self.y + NY - hop, NY)
            self.go_right(chip, hop - 1, q).wait_recv()
            if hop < to_right:
                self.go_right(chip, hop, q).start()
            self.pair(chip, q).start()
        if hop <= to_left:
            chip = lax.rem(self.y + hop, NY)
            self.go_left(chip, hop - 1, q).wait_recv()
            if hop < to_left:
                self.go_left(chip, hop, q).start()
            self.pair(chip, q).start()

    def finish(self, q):
        drain(self.buf.at[pl.ds(0, NY), pl.ds(q * CHUNK, CHUNK)], self.pair_recv.at[q])

    def rows(self, q, count=1):
        return jnp.concatenate(
            [self.buf[k, q * CHUNK : (q + count) * CHUNK] for k in range(TP)], axis=1
        )

    def sent(self):
        drain(self.buf.at[pl.ds(0, NY - 1)], self.send.at[0])
        drain(self.buf.at[pl.ds(0, NY)], self.pair_send.at[0])


def ring_sems(chunks):
    dma = pltpu.SemaphoreType.DMA
    return [dma((1,)), dma((4, chunks)), dma((4, chunks)), dma((1,)), dma((chunks,))]


def kernel(
    query_hbm, forget_hbm, value_hbm, gate_hbm, floor_hbm, head_gain_hbm, proj_hbm,
    tokens_hbm, gain_hbm, routes_hbm, group_hbm, choice_hbm, wg_hbm, wu_hbm, wd_hbm,
    mixer_ref, expert_ref,
    query, forget, value, gate, floor, head_gain, proj, tokens, gain, routes, group,
    choice, wgu, wd, outgoing, back, values, combine_hi, combine_lo, xbuf, hbuf, mbuf,
    x1_send, x1_recv, z2_send, z2_recv, x3_send, incoming,
    load_sem, disp_send, disp_recv, back_sem, mix_sem, *ring_scratch,
):
    z, x = lax.axis_index("z"), lax.axis_index("x")
    y, c = lax.axis_index("y"), lax.axis_index("c")
    me, piece = z * NX + x, y * NC + c

    offsets = [(dz, dx) for dz in range(NZ) for dx in range(NX) if (dz, dx) != (0, 0)]
    far = lambda o: min(o[0], NZ - o[0]) + min(o[1], NX - o[1])
    offsets.sort(key=far, reverse=True)

    def peer(dz, dx):
        return lax.rem(z + dz, NZ), lax.rem(x + dx, NX)

    barrier = pltpu.get_barrier_semaphore()
    for dz, dx in offsets:
        tz, tx = peer(dz, dx)
        pl.semaphore_signal(barrier, inc=1, device_id={"z": tz, "x": tx}, device_id_type=MESH)
    for there in ({"y": lax.rem(y + 1, NY)}, {"y": lax.rem(y + NY - 1, NY)}, {"c": 1 - c}):
        pl.semaphore_signal(barrier, inc=1, device_id=there, device_id_type=MESH)

    loads = [
        pltpu.make_async_copy(src, dst, load_sem.at[k])
        for k, (src, dst) in enumerate(
            [
                (tokens_hbm, tokens), (gain_hbm, gain), (routes_hbm, routes),
                (group_hbm, group), (choice_hbm, choice), (query_hbm, query),
                (forget_hbm, forget), (value_hbm, value), (gate_hbm, gate),
                (floor_hbm, floor), (head_gain_hbm, head_gain),
                (wg_hbm, wgu.at[:, pl.ds(0, LANES)]), (wu_hbm, wgu.at[:, pl.ds(LANES, LANES)]),
                (wd_hbm, wd), (proj_hbm, proj),
            ]
        )
    ]
    for load in loads:
        load.start()

    xring = Ring(xbuf, ring_scratch[0:5], y, c)
    hring = Ring(hbuf, ring_scratch[5:10], y, c)
    mring = Ring(mbuf, ring_scratch[10:15], y, c)

    for load in loads[0:5]:
        load.wait()
    route_rows = [routes[j : j + 1, :] for j in range(2)]
    expert_ids = lax.broadcasted_iota(i32, (EXPERTS, TOKENS_B), 0)
    onehots = [(expert_ids == r).astype(f32) for r in route_rows]
    earlier = (
        lax.broadcasted_iota(i32, (TOKENS_B, TOKENS_B), 0)
        < lax.broadcasted_iota(i32, (TOKENS_B, TOKENS_B), 1)
    ).astype(bf16)
    firsts = nn(onehots[0].astype(bf16), earlier)
    seconds = nn(onehots[1].astype(bf16), earlier) + jnp.sum(onehots[0], axis=1, keepdims=True)
    ranks = [
        jnp.sum(h * n, axis=0, keepdims=True) for h, n in zip(onehots, (firsts, seconds))
    ]
    slot_ids = lax.broadcasted_iota(i32, (SLOTS, TOKENS_B), 0)
    members = [
        slot_ids == r * CAP + n.astype(i32) for r, n in zip(route_rows, ranks)
    ]
    picks = jnp.logical_or(members[0], members[1]).astype(f32).astype(bf16)
    token_rows = tokens[...].astype(f32)
    scale = lax.rsqrt(jnp.mean(token_rows * token_rows, axis=1, keepdims=True) + norm_eps)
    columns = pl.ds(pl.multiple_of(piece * LANES, LANES), LANES)
    normed = (tokens[:, columns].astype(f32) * scale * gain[:, columns]).astype(bf16)
    outgoing[...] = nn(picks, normed).astype(bf16)

    pl.semaphore_wait(barrier, len(offsets) + 3)
    for dz, dx in offsets:
        tz, tx = peer(dz, dx)
        there = tz * NX + tx
        remote(
            outgoing.at[pl.ds(there * CAP, CAP)],
            xbuf.at[piece, pl.ds(me * CAP, CAP)],
            disp_send.at[0],
            disp_recv.at[z // 2],
            z=tz,
            x=tx,
        ).start()
    mine = pl.ds(pl.multiple_of(me * CAP, CAP), CAP)
    xbuf[piece, mine] = outgoing[mine, :]

    for load in loads[5:11]:
        load.wait()
    query_pre = query[...].astype(f32)
    queries = query_pre * sigmoid(query_pre)
    rates = (1.0 - floor[...]) * sigmoid(-forget[...].astype(f32))
    log_forget = jnp.log1p(-rates)
    row_ids = lax.broadcasted_iota(i32, (TOKENS_A, TOKENS_A), 0)
    col_ids = lax.broadcasted_iota(i32, (TOKENS_A, TOKENS_A), 1)
    causal = col_ids <= row_ids
    triangle = causal.astype(f32).astype(bf16)
    log_hi = log_forget.astype(bf16)
    log_mid, log_lo = halves(log_forget - log_hi.astype(f32))
    total = nn(triangle, log_hi) + (nn(triangle, log_mid) + nn(triangle, log_lo))
    last = total[TOKENS_A - 1 : TOKENS_A, :]
    keys_end = rates * jnp.exp(last - total)
    value_t = jnp.transpose(value[...].astype(f32)).astype(bf16)
    end_hi, end_lo = halves(keys_end)
    state = nn(value_t, end_hi) + nn(value_t, end_lo)
    last_hi = last.astype(bf16)
    last_mid, last_lo = halves(last - last_hi.astype(f32))

    def pack(ref, part, logs):
        hi = logs.astype(bf16)
        mid, lo = halves(logs - hi.astype(f32))
        rows = jnp.concatenate(
            [part, hi.astype(f32), mid.astype(f32), lo.astype(f32),
             jnp.zeros((MSG - SLICE - 3, LANES), f32)], axis=0)
        ref[...] = rows.astype(bf16)

    def unpack(msg):
        rows = msg.astype(f32)
        logs = rows[SLICE : SLICE + 1] + rows[SLICE + 1 : SLICE + 2] + rows[SLICE + 2 : SLICE + 3]
        return rows[0:SLICE], logs

    for k in range(NX):
        pack(x1_send.at[k], state[k * SLICE : (k + 1) * SLICE], last)
    for d in range(1, NX):
        tx = lax.rem(x + d, NX)
        remote(x1_send.at[tx], x1_recv.at[x], mix_sem.at[0], mix_sem.at[1], x=tx).start()
    x1_recv[x] = x1_send[x]

    queries_hi, queries_lo = halves(queries * jnp.exp(total))
    keys_hi, keys_lo = halves(rates * jnp.exp(-total))
    scores = nt(queries_hi, keys_hi) + (nt(queries_hi, keys_lo) + nt(queries_lo, keys_hi))
    scores_hi, scores_lo = halves(jnp.where(causal, scores, 0.0))
    inner = nn(scores_hi, value[...]) + nn(scores_lo, value[...])
    gate_pre = gate[...].astype(f32)
    gate_act = gate_pre * sigmoid(gate_pre) * head_gain[...]

    drain(x1_recv.at[pl.ds(0, NX - 1)], mix_sem.at[1])
    parts = [unpack(x1_recv[k]) for k in range(NX)]
    before = [(jnp.zeros((SLICE, LANES), f32), jnp.zeros((1, LANES), f32))]
    for part, logs in parts:
        so_far, log_so_far = before[-1]
        before.append((jnp.exp(logs) * so_far + part, log_so_far + logs))
    pack(z2_send, *before[NX])
    for d in range(1, NZ):
        tz = lax.rem(z + d, NZ)
        remote(z2_send, z2_recv.at[z], mix_sem.at[2], mix_sem.at[3], z=tz).start()
    z2_recv[z] = z2_send[...]

    group_exp = jnp.exp(group[...])
    group_prob = group_exp / jnp.sum(group_exp, axis=0, keepdims=True)
    groups_of = [r // EXP_GROUP for r in route_rows]
    group_ids = lax.broadcasted_iota(i32, (GROUPS, TOKENS_B), 0)
    picked = [
        jnp.sum(jnp.where(group_ids == g, group_prob, 0.0), axis=0, keepdims=True)
        for g in groups_of
    ]
    choice_exp = jnp.exp(choice[...])
    exps = [choice_exp[j : j + 1] for j in range(2)]
    together = (groups_of[0] == groups_of[1]).astype(f32)
    weights = [
        picked[0] * exps[0] / (exps[0] + together * exps[1]),
        picked[1] * exps[1] / (exps[1] + together * exps[0]),
    ]
    spread = jnp.where(members[0], weights[0], 0.0) + jnp.where(members[1], weights[1], 0.0)
    combine = jnp.transpose(spread)
    high, low = halves(combine)
    combine_hi[...] = high
    combine_lo[...] = low

    chunks = SLOTS // CHUNK
    own = z // 2
    for q in range(chunks):
        rows = q * CHUNK

        @pl.when(own == q)
        def _():
            drain(outgoing.at[pl.ds(rows, CHUNK - CAP)], disp_recv.at[q])

        @pl.when(own != q)
        def _():
            drain(outgoing.at[pl.ds(rows, CHUNK)], disp_recv.at[q])

        xring.start(q)
    for q in range(chunks):
        xring.step(1, q)

    drain(z2_recv.at[pl.ds(0, NZ - 1)], mix_sem.at[3])
    prefix = jnp.zeros((SLICE, LANES), f32)
    for k in range(NZ):
        part, logs = unpack(z2_recv[k])
        prefix = jnp.where(k < z, jnp.exp(logs) * prefix + part, prefix)
    for k in range(NX):
        x3_send[k] = (jnp.exp(before[k][1]) * prefix + before[k][0]).astype(bf16)
    mine3 = pl.ds(pl.multiple_of(x * SLICE, SLICE), SLICE)
    for d in range(1, NX):
        tx = lax.rem(x + d, NX)
        remote(x3_send.at[tx], incoming.at[mine3], mix_sem.at[4], mix_sem.at[5], x=tx).start()
    incoming[mine3, :] = x3_send[x]

    for q in range(chunks):
        xring.step(2, q)

    drain(incoming.at[pl.ds(0, LANES - SLICE)], mix_sem.at[5])
    state_in = incoming[...]
    recurrent = inner + (nt(queries_hi, state_in) + nt(queries_lo, state_in))
    size = lax.rsqrt(jnp.mean(recurrent * recurrent, axis=1, keepdims=True) + norm_eps)
    mbuf[piece] = (recurrent * size * gate_act).astype(bf16)

    for q in range(chunks):
        xring.step(3, q)
    for q in range(TOKENS_A // CHUNK):
        mring.start(q)
    loads[11].wait()
    loads[12].wait()
    for q in range(chunks):
        xring.step(4, q)
        xring.finish(q)
        both = nn(xring.rows(q), wgu[...])
        pre = both[:, 0:LANES]
        hbuf[piece, q * CHUNK : (q + 1) * CHUNK] = (pre * sigmoid(pre) * both[:, LANES:]).astype(bf16)
        hring.start(q)
    for q in range(TOKENS_A // CHUNK):
        mring.step(1, q)
    for hop in (1, 2, 3):
        for q in range(chunks):
            hring.step(hop, q)
    for q in range(TOKENS_A // CHUNK):
        mring.step(2, q)
    loads[13].wait()
    for q in range(chunks):
        hring.step(4, q)
        hring.finish(q)
        values[q * CHUNK : (q + 1) * CHUNK] = nn(hring.rows(q), wd[...]).astype(bf16)
        for s in range(q * CHUNK // CAP, (q + 1) * CHUNK // CAP):
            sz, sx = s // NX, s % NX

            @pl.when(me != s)
            def _():
                remote(
                    values.at[pl.ds(s * CAP, CAP)],
                    back.at[pl.ds(me * CAP, CAP)],
                    back_sem.at[0],
                    back_sem.at[1],
                    z=sz,
                    x=sx,
                ).start()

            @pl.when(me == s)
            def _():
                back[s * CAP : (s + 1) * CAP] = values[s * CAP : (s + 1) * CAP]

    for hop in (3, 4):
        for q in range(TOKENS_A // CHUNK):
            mring.step(hop, q)
    loads[14].wait()
    for q in range(TOKENS_A // CHUNK):
        mring.finish(q)
    mixer_ref[...] = nn(mring.rows(0, TOKENS_A // CHUNK), proj[...]).astype(bf16)

    drain(back.at[pl.ds(0, SLOTS - CAP)], back_sem.at[1])
    returned = back[...]
    expert_ref[...] = (nn(combine_hi[...], returned) + nn(combine_lo[...], returned)).astype(bf16)

    drain(outgoing.at[pl.ds(0, SLOTS - CAP)], disp_send.at[0])
    drain(values.at[pl.ds(0, SLOTS - CAP)], back_sem.at[0])
    drain(x1_recv.at[pl.ds(0, NX - 1)], mix_sem.at[0])
    drain(z2_recv.at[pl.ds(0, NZ - 1)], mix_sem.at[2])
    drain(x3_send.at[pl.ds(0, NX - 1)], mix_sem.at[4])
    for ring in (xring, hring, mring):
        ring.sent()


def per_device(
    mixer_query, mixer_forget, mixer_value, mixer_gate, forget_floor, head_gain, mixer_proj,
    expert_tokens, expert_gain, routes, group_logits, choice_logits, w_gate, w_up, w_down,
):
    vmem, dma = pltpu.VMEM, pltpu.SemaphoreType.DMA
    args = (
        mixer_query, mixer_forget, mixer_value, mixer_gate,
        forget_floor.reshape(1, -1), head_gain.reshape(1, -1), mixer_proj,
        expert_tokens, expert_gain.reshape(1, -1),
        routes.T, group_logits.T, choice_logits.T,
        w_gate[0], w_up[0], w_down[0],
    )
    chunks = SLOTS // CHUNK
    scratch = [vmem(a.shape, a.dtype) for a in args[0:12]]
    scratch += [
        vmem((WIDTH, 2 * LANES), bf16),
        vmem((WIDTH, LANES), bf16),
        vmem((SLOTS, LANES), bf16),
        vmem((SLOTS, LANES), bf16),
        vmem((SLOTS, LANES), bf16),
        vmem((TOKENS_B, SLOTS), bf16),
        vmem((TOKENS_B, SLOTS), bf16),
        vmem((TP, SLOTS, LANES), bf16),
        vmem((TP, SLOTS, LANES), bf16),
        vmem((TP, TOKENS_A, LANES), bf16),
        vmem((NX, MSG, LANES), bf16),
        vmem((NX, MSG, LANES), bf16),
        vmem((MSG, LANES), bf16),
        vmem((NZ, MSG, LANES), bf16),
        vmem((NX, SLICE, LANES), bf16),
        vmem((LANES, LANES), bf16),
        dma((len(args),)),
        dma((1,)),
        dma((chunks,)),
        dma((2,)),
        dma((6,)),
    ]
    scratch += ring_sems(chunks) + ring_sems(chunks) + ring_sems(TOKENS_A // CHUNK)
    return pl.pallas_call(
        kernel,
        out_shape=(
            jax.ShapeDtypeStruct((TOKENS_A, LANES), bf16),
            jax.ShapeDtypeStruct((TOKENS_B, LANES), bf16),
        ),
        in_specs=[pl.BlockSpec(memory_space=pltpu.HBM)] * len(args),
        out_specs=(pl.BlockSpec(memory_space=vmem), pl.BlockSpec(memory_space=vmem)),
        scratch_shapes=scratch,
        compiler_params=pltpu.CompilerParams(
            collective_id=0, has_side_effects=True, vmem_limit_bytes=40 << 20
        ),
        name="hybrid_layer",
    )(*args)


def solution(mesh):
    finer = Mesh(mesh.devices.reshape(NZ, NX, NY, NC), ("z", "x", "y", "c"))
    ep, tp = ("z", "x"), ("y", "c")
    placed = (
        P(ep, tp),
        P(ep, tp),
        P(ep, tp),
        P(ep, tp),
        P(tp),
        P(),
        P(None, tp),
        P(ep, None),
        P(),
        P(ep, None),
        P(ep, None),
        P(ep, None),
        P(ep, None, tp),
        P(ep, None, tp),
        P(ep, None, tp),
    )
    return jax.shard_map(
        per_device,
        mesh=finer,
        in_specs=placed,
        out_specs=(P(ep, tp), P(ep, tp)),
        check_vma=False,
    )
```

time: 174 us -> 75.2 us (0.43)
  Pallas kernels: 0 us -> 63.4 us
  waiting for transfers between devices: 62.6 us -> 0 us
  blocking collectives: 31.2 us -> 0 us
  starting transfers between devices: 28.9 us -> 0 us
  other arithmetic: 14.2 us -> 0 us
  between operations: 14.4 us -> 0.7 us
  matrix products: 12.9 us -> 0 us
    pallas_call x0 -> x1, Pallas kernels: none -> 63.4 us  [per_device(): pl.pallas_call(kernel, out_shape=(jax.ShapeDtypeStruct((TOKENS_A, LANES),...]
    all_to_all x3 -> x0, waiting for transfers between devices: 50 us -> none  [the longest x1 26.2 us: from_everyone(): return lax.all_to_all(copies, axis, split_axis=0, concat_axis=0, tiled=True)]
    all_gather x2 -> x0, blocking collectives: 31.2 us -> none  [collected_together(): both, at, found = (lax.all_gather(jnp.concatenate(lines), axis), 0, {})]
    all_to_all x3 -> x0, starting transfers between devices: 28.8 us -> none  [the longest x1 13.8 us: expert_local(): lax.all_to_all(outgoing, EP, split_axis=0, concat_axis=0, tiled=True)]
    dot_general x17 -> x0, matrix products: 12.9 us -> none  [the longest x4 3.09 us: block_terms(): jnp.einsum('tsh,shv->thv', scores, value_block, precision=highest_precision)]
    all_gather x1 -> x0, waiting for transfers between devices: 12.6 us -> none  [mixer_local(): lax.all_gather(mixed_heads, 'tp', axis=1, tiled=True)]
    unnamed x23 -> x32, local copies, waits for them, and re-layouts: 0.9 us -> 10.5 us
    reduce_sum x10 -> x0, other arithmetic: 7.66 us -> none  [the longest x4 5.4 us: block_terms(): jnp.sum(query_block[:, None] * input_block[None, :] * decays, axis=-1)]
  transfers between devices with their start and end apart: 4 -> 0, of which waited for: 3 -> 0; matrix products, arithmetic and copies ran while one was open for 12% -> 0% of each run, Pallas kernels for 0% -> 0%
where the time goes in v1:
time: 75.2 us; the launch traced here: 74.6 us
  Pallas kernels  63.4 us (84%)
  local copies, waits for them, and re-layouts  10.5 us (14%)
    pallas_call x1, Pallas kernels, per_device(): pl.pallas_call(kernel, out_shape=(jax.ShapeDtypeStruct((TOKENS_A, LANES),...  63.4 us
    unnamed x32, local copies, waits for them, and re-layouts  10.5 us

profile of v1, /device:TPU:1, one launch (start us, length us, event | category | flops | bytes accessed | tf_op | source)
XLA Modules:
  0.0 74.6 jit_solution(7483938166898641442)
XLA Ops:
  0.6 0.0 copy-start.9
  0.6 0.0 copy-start.12
  0.7 0.0 copy-start.14
  0.7 0.0 copy-start.10
  0.7 0.0 copy-start.11
  0.7 0.0 copy-start.13
  0.7 0.6 copy-done.9
  1.3 0.0 copy-done.12
  1.3 0.0 copy-done.14
  1.3 0.0 copy-done.10
  1.4 0.0 copy-done.11
  1.4 0.0 copy-done.13
  1.4 0.0 copy-start
  1.4 1.0 %copy-done = bf16[2048,128]{1,0:T(8,128)(2,1)S(1)} copy-done((bf16[2048,128]{1,0:T(8,128)(2,1)S(1)}, bf16[2048,128]{1,0:T(8,128)(2,1)}, u32[]{:S(2)}) %copy-start) | copy-done | bytes 524312
  2.4 0.0 copy-start.1
  2.4 1.0 %copy-done.1 = bf16[128,2048]{1,0:T(8,128)(2,1)S(1)} copy-done((bf16[128,2048]{1,0:T(8,128)(2,1)S(1)}, bf16[128,2048]{1,0:T(8,128)(2,1)}, u32[]{:S(2)}) %copy-start.1) | copy-done | bytes 524312
  3.5 0.0 copy-start.2
  3.5 1.0 %copy-done.2 = bf16[1,2048,128]{2,1,0:T(8,128)(2,1)S(1)} copy-done((bf16[1,2048,128]{2,1,0:T(8,128)(2,1)S(1)}, bf16[1,2048,128]{2,1,0:T(8,128)(2,1)}, u32[]{:S(2)}) %copy-start.2) | copy-done | bytes 524312
  4.5 0.0 copy-start.3
  4.5 1.0 %copy-done.3 = bf16[1,2048,128]{2,1,0:T(8,128)(2,1)S(1)} copy-done((bf16[1,2048,128]{2,1,0:T(8,128)(2,1)S(1)}, bf16[1,2048,128]{2,1,0:T(8,128)(2,1)}, u32[]{:S(2)}) %copy-start.3) | copy-done | bytes 524312
  5.6 0.0 copy-start.4
  5.6 1.0 %copy-done.4 = bf16[1,2048,128]{2,1,0:T(8,128)(2,1)S(1)} copy-done((bf16[1,2048,128]{2,1,0:T(8,128)(2,1)S(1)}, bf16[1,2048,128]{2,1,0:T(8,128)(2,1)}, u32[]{:S(2)}) %copy-start.4) | copy-done | bytes 524312
  6.6 0.0 copy-start.5
  6.6 0.8 %copy-done.5 = bf16[256,128]{1,0:T(8,128)(2,1)S(1)} copy-done((bf16[256,128]{1,0:T(8,128)(2,1)S(1)}, bf16[256,128]{1,0:T(8,128)(2,1)}, u32[]{:S(2)}) %copy-start.5) | copy-done | bytes 65560
  7.4 0.0 copy-start.6
  7.4 0.8 %copy-done.6 = bf16[256,128]{1,0:T(8,128)(2,1)S(1)} copy-done((bf16[256,128]{1,0:T(8,128)(2,1)S(1)}, bf16[256,128]{1,0:T(8,128)(2,1)}, u32[]{:S(2)}) %copy-start.6) | copy-done | bytes 65560
  8.3 0.0 copy-start.7
  8.3 0.8 %copy-done.7 = bf16[256,128]{1,0:T(8,128)(2,1)S(1)} copy-done((bf16[256,128]{1,0:T(8,128)(2,1)S(1)}, bf16[256,128]{1,0:T(8,128)(2,1)}, u32[]{:S(2)}) %copy-start.7) | copy-done | bytes 65560
  9.1 0.0 copy-start.8
  9.1 0.8 %copy-done.8 = bf16[256,128]{1,0:T(8,128)(2,1)S(1)} copy-done((bf16[256,128]{1,0:T(8,128)(2,1)S(1)}, bf16[256,128]{1,0:T(8,128)(2,1)}, u32[]{:S(2)}) %copy-start.8) | copy-done | bytes 65560
  10.0 63.4 %hybrid_layer.1 = (bf16[256,128]{1,0:T(8,128)(2,1)S(1)}, bf16[128,128]{1,0:T(8,128)(2,1)S(1)}) custom-call(bf16[256,128]{1,0:T(8,128)(2,1)S(1)} %copy-done.5, bf16[256,128]{1,0:T(8,128)(2,1)S(1)} %copy-done.6, bf16[256,128]{1,0:T(8,128)(2,1)S(1)} %copy-done.7, bf16[256,128]{1,0:T(8,128)(2,1)S(1)} %copy-done.8, f32[1,128]{1,0:T(1,128)S(1)} %bitcast.16, ...), custom_call_target="tpu_custom_call" | custom-call | tf_op jit(solution)/shard_map/hybrid_layer/pallas_call | solution.py:434
  73.3 0.6 copy.19
  74.0 0.6 copy.20
Async XLA Ops:
  0.6 0.7 copy-start.9
  0.6 0.7 copy-start.12
  0.7 0.7 copy-start.14
  0.7 0.7 copy-start.10
  0.7 0.7 copy-start.11
  0.7 0.7 copy-start.13
  1.4 1.0 %copy-start = (bf16[2048,128]{1,0:T(8,128)(2,1)S(1)}, bf16[2048,128]{1,0:T(8,128)(2,1)}, u32[]{:S(2)}) copy-start(bf16[2048,128]{1,0:T(8,128)(2,1)} %proj_hbm.1) | copy-start | bytes 1572868
  2.4 1.0 %copy-start.1 = (bf16[128,2048]{1,0:T(8,128)(2,1)S(1)}, bf16[128,2048]{1,0:T(8,128)(2,1)}, u32[]{:S(2)}) copy-start(bf16[128,2048]{1,0:T(8,128)(2,1)} %tokens_hbm.1) | copy-start | bytes 1572868
  3.5 1.0 %copy-start.2 = (bf16[1,2048,128]{2,1,0:T(8,128)(2,1)S(1)}, bf16[1,2048,128]{2,1,0:T(8,128)(2,1)}, u32[]{:S(2)}) copy-start(bf16[1,2048,128]{2,1,0:T(8,128)(2,1)} %param.27) | copy-start | bytes 1572868
  4.5 1.0 %copy-start.3 = (bf16[1,2048,128]{2,1,0:T(8,128)(2,1)S(1)}, bf16[1,2048,128]{2,1,0:T(8,128)(2,1)}, u32[]{:S(2)}) copy-start(bf16[1,2048,128]{2,1,0:T(8,128)(2,1)} %param.28) | copy-start | bytes 1572868
  5.6 1.0 %copy-start.4 = (bf16[1,2048,128]{2,1,0:T(8,128)(2,1)S(1)}, bf16[1,2048,128]{2,1,0:T(8,128)(2,1)}, u32[]{:S(2)}) copy-start(bf16[1,2048,128]{2,1,0:T(8,128)(2,1)} %param.29) | copy-start | bytes 1572868
  6.6 0.8 %copy-start.5 = (bf16[256,128]{1,0:T(8,128)(2,1)S(1)}, bf16[256,128]{1,0:T(8,128)(2,1)}, u32[]{:S(2)}) copy-start(bf16[256,128]{1,0:T(8,128)(2,1)} %query_hbm.1) | copy-start | bytes 196612
  7.4 0.8 %copy-start.6 = (bf16[256,128]{1,0:T(8,128)(2,1)S(1)}, bf16[256,128]{1,0:T(8,128)(2,1)}, u32[]{:S(2)}) copy-start(bf16[256,128]{1,0:T(8,128)(2,1)} %forget_hbm.1) | copy-start | bytes 196612
  8.3 0.8 %copy-start.7 = (bf16[256,128]{1,0:T(8,128)(2,1)S(1)}, bf16[256,128]{1,0:T(8,128)(2,1)}, u32[]{:S(2)}) copy-start(bf16[256,128]{1,0:T(8,128)(2,1)} %value_hbm.1) | copy-start | bytes 196612
  9.1 0.8 %copy-start.8 = (bf16[256,128]{1,0:T(8,128)(2,1)S(1)}, bf16[256,128]{1,0:T(8,128)(2,1)}, u32[]{:S(2)}) copy-start(bf16[256,128]{1,0:T(8,128)(2,1)} %gate_hbm.1) | copy-start | bytes 196612
